TPU v7x, 32 devices: a whole 2x2x4 slice. The times are simulated.
32 devices in a mesh: sp: 8 (over z, y), tp: 4 (over x, core).
Axes of the slice: x: 2, y: 2, z: 4, core: 2. Of those that a mesh axis runs over, the one named last changes fastest.
Arguments:
- residual: bfloat16 [8192, 2048], P('sp'), may hold values from -6 to 6
- small_heads: bfloat16 [8192, 1024], P('sp', 'tp'), may hold values from -6 to 6
- large_heads: bfloat16 [8192, 1024], P('sp', 'tp'), may hold values from -6 to 6
- state_keys: bfloat16 [8192, 8, 128], P('sp', 'tp'), may hold values from -6 to 6
- state_queries: bfloat16 [8192, 8, 128], P('sp', 'tp'), may hold values from -6 to 6
- small_gate: bfloat16 [8192, 1024], P('sp', 'tp'), may hold values from -6 to 6
- large_gate: bfloat16 [8192, 1024], P('sp', 'tp'), may hold values from -6 to 6
- small_step: float32 [8192, 16], P('sp', 'tp'), may hold values from -3 to 2
- large_step: float32 [8192, 8], P('sp', 'tp'), may hold values from -3 to 2
- small_taps: bfloat16 [4, 1024], P(None, 'tp'), may hold values from -3 to 3
- large_taps: bfloat16 [4, 1024], P(None, 'tp'), may hold values from -3 to 3
- key_taps: bfloat16 [4, 8, 128], P(None, 'tp'), may hold values from -3 to 3
- query_taps: bfloat16 [4, 8, 128], P(None, 'tp'), may hold values from -3 to 3
- small_decay: float32 [16], P('tp'), may hold values from -12 to -2, as said below
- large_decay: float32 [8], P('tp'), may hold values from -12 to -2, as said below
- small_gain: bfloat16 [1024], P('tp'), may hold values from 0.099609375 to 1.8984375
- large_gain: bfloat16 [1024], P('tp'), may hold values from 0.099609375 to 1.8984375
- small_out: bfloat16 [1024, 2048], P('tp'), may hold values from -0.125 to 0.125
- large_out: bfloat16 [1024, 2048], P('tp'), may hold values from -0.125 to 0.125
- mixer_gain: bfloat16 [2048], replicated, may hold values from 0.099609375 to 1.8984375
- ffn_in_gain: bfloat16 [2048], replicated, may hold values from 0.099609375 to 1.8984375
- gate_proj: bfloat16 [2048, 5632], P('sp', 'tp'), may hold values from -0.125 to 0.125
- up_proj: bfloat16 [2048, 5632], P('sp', 'tp'), may hold values from -0.125 to 0.125
- down_proj: bfloat16 [2048, 5632], P('sp', 'tp'), may hold values from -0.078125 to 0.078125
- ffn_out_gain: bfloat16 [2048], replicated, may hold values from 0.099609375 to 1.8984375
Outputs:
- updated: bfloat16 [8192, 2048], P(('sp', 'tp'))
Inputs may be any that keep to these rules, and one draw needn't show every extreme that they name: `small_decay`: log decay rates of the first group. `large_decay`: log decay rates of the second group.
All inputs are finite; a program needn't handle non-finite values.
Results may differ from a plain program's by a relative error of at most 0.014.
Values may be sent and summed in bfloat16 or wider, within the bound.
A program may use at most 192 MiB of HBM per device.

v0:
```python
import functools

import jax
import jax.numpy as jnp
from jax import lax
from jax.experimental import pallas as pl
from jax.experimental.pallas import tpu as pltpu
from jax.sharding import PartitionSpec as P


BLOCK = 128
HALO = 16
LANES = 128
SLOTS = 8
TAIL = 16


EPS = 1e-06
OUTER, INNER, PARTS = "so", "si", 2
SEQ = (OUTER, INNER)
FAR = -1e30
F32 = jnp.float32
BF16 = jnp.bfloat16


def moved(block, axis, route):
    return lax.ppermute(block, axis, route)


def earlier(block, axis, distance):
    devices = range(lax.axis_size(axis))
    return moved(block, axis, [(i - distance, i) for i in devices if i - distance in devices])


def paired(block, axis, bit):
    return moved(block, axis, [(i, i ^ bit) for i in range(lax.axis_size(axis))])


def silu(x):
    return x / (1.0 + jnp.exp(-x))


def softplus(x):
    return jnp.maximum(x, 0.0) + jnp.log1p(jnp.exp(-jnp.abs(x)))


def exact_dot(a, b):
    return lax.dot_general(
        a, b, (((1,), (0,)), ((), ())), precision=lax.Precision.HIGHEST, preferred_element_type=F32
    )


def lower(n):
    rows = lax.broadcasted_iota(jnp.int32, (n, n), 0)
    return rows >= lax.broadcasted_iota(jnp.int32, (n, n), 1)


def spread(columns, heads, dim):
    rows = columns.shape[0]
    parts = []
    if dim >= LANES:
        for h in heads:
            parts.append(jnp.broadcast_to(columns[:, h : h + 1], (rows, dim)))
    else:
        per = LANES // dim
        lane = lax.broadcasted_iota(jnp.int32, (rows, LANES), 1)
        for first in range(0, len(heads), per):
            part = jnp.broadcast_to(columns[:, heads[first] : heads[first] + 1], (rows, LANES))
            for j in range(1, per):
                h = heads[first + j]
                part = jnp.where(lane >= j * dim, columns[:, h : h + 1], part)
            parts.append(part)
    return jnp.concatenate(parts, axis=1)


def conv_kernel(
    sizes, small, large, keys, queries, halo, taps, steps, decay, conv, packed, before, state, total
):
    (heads_a, dim_a), (heads_b, dim_b), state_len = sizes
    step = pl.program_id(0)

    @pl.when(step == 0)
    def _():
        before[...] = halo[...]
        state[...] = jnp.zeros_like(state)
        total[...] = jnp.zeros_like(total)

    column = 0
    for ref in (small, large, keys, queries):
        width = ref.shape[1]
        for start in range(0, width, LANES):
            here = pl.ds(column, LANES)
            now = ref[:, pl.ds(start, LANES)]
            extended = jnp.concatenate([before[:, here], now], axis=0).astype(F32)
            kernel_len = taps.shape[0]
            summed = None
            for k in range(kernel_len):
                first = HALO - kernel_len + 1 + k
                term = taps[k : k + 1, here] * extended[first : first + BLOCK]
                summed = term if summed is None else summed + term
            done = silu(summed).astype(BF16)
            conv[:, here] = done
            before[:, here] = now[BLOCK - HALO :]
            column += LANES
    dt = softplus(steps[...])
    cum = exact_dot(lower(BLOCK).astype(F32), -dt * jnp.exp(decay[...]))
    tail = cum[BLOCK - 1 : BLOCK]
    scale = dt * jnp.exp(tail - cum)
    head_list_a = list(range(heads_a))
    head_list_b = list(range(heads_a, heads_a + heads_b))
    kept = jnp.exp(tail)
    offset = 0
    width_a = heads_a * dim_a
    width_b = heads_b * dim_b
    for heads, dim, width, key_at in (
        (head_list_a, dim_a, width_a, width_a + width_b),
        (head_list_b, dim_b, width_b, width_a + width_b + state_len),
    ):
        x = conv[:, offset : offset + width].astype(F32)
        u = (x * spread(scale, heads, dim)).astype(BF16)
        k = conv[:, key_at : key_at + state_len]
        fresh = lax.dot_general(k, u, (((0,), (0,)), ((), ())), preferred_element_type=F32)
        old = state[:, offset : offset + width]
        state[:, offset : offset + width] = old * spread(kept, heads, dim) + fresh
        offset += width
    total[...] = total[...] + tail

    @pl.when(step == pl.num_programs(0) - 1)
    def _():
        packed[:state_len] = state[...].astype(BF16)
        whole = jnp.concatenate(
            [spread(total[...], head_list_a, dim_a), spread(total[...], head_list_b, dim_b)], axis=1
        )
        high = whole.astype(BF16)
        low = (whole - high.astype(F32)).astype(BF16)
        row = lax.broadcasted_iota(jnp.int32, (TAIL, whole.shape[1]), 0)
        both = jnp.where(row == 0, high.astype(F32), jnp.where(row == 1, low.astype(F32), 0.0))
        packed[state_len:] = both.astype(BF16)


def mix_kernel(
    sizes,
    place,
    conv,
    small_gate,
    large_gate,
    steps,
    steps_across,
    decay,
    decay_across,
    gain,
    small_out,
    large_out,
    entering,
    partial_out,
    state,
):
    (heads_a, dim_a), (heads_b, dim_b), state_len = sizes
    step = pl.program_id(0)

    @pl.when(step == 0)
    def _():
        state[...] = entering[...]

    causal = lower(BLOCK)
    ones = causal.astype(F32)
    dt = softplus(steps[...])
    cum = exact_dot(ones, -dt * jnp.exp(decay[...]))
    dt_across = softplus(steps_across[...])
    upper = (
        lax.broadcasted_iota(jnp.int32, (BLOCK, BLOCK), 0)
        <= lax.broadcasted_iota(jnp.int32, (BLOCK, BLOCK), 1)
    ).astype(F32)
    cum_across = exact_dot(-dt_across * jnp.exp(decay_across[...]), upper)
    tail = cum[BLOCK - 1 : BLOCK]
    scale = dt * jnp.exp(tail - cum)
    grown = jnp.exp(cum)
    kept = jnp.exp(tail)
    width_a = heads_a * dim_a
    width_b = heads_b * dim_b
    offset = 0
    result = None
    lane = lax.broadcasted_iota(jnp.int32, (BLOCK, LANES), 1)
    for which, (heads, dim, width, gate, out) in enumerate(
        (
            (list(range(heads_a)), dim_a, width_a, small_gate, small_out),
            (list(range(heads_a, heads_a + heads_b)), dim_b, width_b, large_gate, large_out),
        )
    ):
        key_at = width_a + width_b + which * state_len
        query_at = key_at + 2 * state_len
        x = conv[:, offset : offset + width]
        k = conv[:, key_at : key_at + state_len]
        q = conv[:, query_at : query_at + state_len]
        scores = lax.dot_general(q, k, (((1,), (1,)), ((), ())), preferred_element_type=F32)
        old = state[:, offset : offset + width]
        carried = jnp.dot(q, old.astype(BF16), preferred_element_type=F32)
        carried = carried * spread(grown, heads, dim)
        u = (x.astype(F32) * spread(scale, heads, dim)).astype(BF16)
        fresh = lax.dot_general(k, u, (((0,), (0,)), ((), ())), preferred_element_type=F32)
        state[:, offset : offset + width] = old * spread(kept, heads, dim) + fresh
        inside = []
        span = max(dim, LANES)
        per = span // dim
        for first in range(0, len(heads), per):
            x_part = x[:, first * dim : first * dim + span]
            part = None
            for j in range(per):
                h = heads[first + j]
                gap = cum[:, h : h + 1] - cum_across[h : h + 1]
                decays = jnp.exp(jnp.where(causal, gap, FAR))
                w = (scores * decays * dt_across[h : h + 1]).astype(BF16)
                got = jnp.dot(w, x_part, preferred_element_type=F32)
                part = got if part is None else jnp.where(lane >= j * dim, got, part)
            inside.append(part)
        mixed = jnp.concatenate(inside, axis=1) + carried
        gated = mixed * silu(gate[...].astype(F32))
        squares = gated * gated
        normed = []
        for first in range(0, len(heads), per):
            at = first * dim
            part = squares[:, at : at + span]
            means = None
            for j in range(per):
                if per == 1:
                    means = jnp.sum(part, axis=1, keepdims=True)
                else:
                    ours = (lane >= j * dim) & (lane < (j + 1) * dim)
                    one = jnp.sum(jnp.where(ours, part, 0.0), axis=1, keepdims=True)
                    means = one if means is None else jnp.where(lane >= j * dim, one, means)
            normed.append(gated[:, at : at + span] * lax.rsqrt(means * (1.0 / dim) + EPS))
        normed = jnp.concatenate(normed, axis=1) * gain[:, offset : offset + width]
        product = jnp.dot(normed.astype(BF16), out[...], preferred_element_type=F32)
        result = product if result is None else result + product
        offset += width
    partial_out[...] = result.astype(BF16)[None]


def unit_rms(values):
    return values * lax.rsqrt(jnp.mean(values * values, axis=-1, keepdims=True) + EPS)


def reversed_bits(value, count):
    out = 0
    bit = 1
    while bit < count:
        out = out * 2 + (value // bit) % 2
        bit *= 2
    return out


def scattered(blocks, axis):
    bit = 1
    while blocks.shape[0] > 1:
        half = blocks.shape[0] // 2
        other = paired(blocks[half:], axis, bit)
        total = blocks[:half].astype(F32) + other.astype(F32)
        bit *= 2
        blocks = total if half == 1 else total.astype(BF16)
    return blocks[0].astype(F32)


def collected(block, axis):
    blocks = block[None]
    bit = lax.axis_size(axis) // 2
    while bit >= 1:
        other = paired(blocks, axis, bit)
        blocks = jnp.concatenate([blocks, other], axis=0)
        bit //= 2
    return blocks


def layer(
    residual,
    small_heads,
    large_heads,
    state_keys,
    state_queries,
    small_gate,
    large_gate,
    small_step,
    large_step,
    small_taps,
    large_taps,
    key_taps,
    query_taps,
    small_decay,
    large_decay,
    small_gain,
    large_gain,
    small_out,
    large_out,
    mixer_gain,
    ffn_in_gain,
    gate_proj,
    up_proj,
    down_proj,
    ffn_out_gain,
):
    length, features = residual.shape
    state_len = state_keys.shape[-1]
    key_rows = state_keys.reshape(length, -1)
    query_rows = state_queries.reshape(length, -1)
    halo_rows = small_taps.shape[0] - 1
    first_row = length - halo_rows
    last = jnp.concatenate(
        [a[first_row:] for a in (small_heads, large_heads, key_rows, query_rows)], axis=1
    )
    halo = earlier(last, SEQ, 1)
    halo = jnp.pad(halo, ((HALO - halo_rows, 0), (0, 0)))
    side = lax.axis_index(INNER)
    down_other = paired(down_proj, INNER, 1)
    down_pair = jnp.where(
        side == 0, jnp.stack([down_proj, down_other]), jnp.stack([down_other, down_proj])
    )
    gate_mine = lax.all_gather(gate_proj, OUTER, axis=0, tiled=True)
    up_mine = lax.all_gather(up_proj, OUTER, axis=0, tiled=True)
    own_rows = down_proj.shape[0]
    piece = own_rows // PARTS
    down_parts = []
    for p in range(PARTS):
        sent = down_pair[:, p * piece : (p + 1) * piece].reshape(2 * piece, -1)
        down_parts.append(lax.all_gather(sent, OUTER, axis=0, tiled=True))
    gate_theirs = paired(gate_mine, INNER, 1)
    up_theirs = paired(up_mine, INNER, 1)

    heads_a = small_step.shape[1]
    heads_b = large_step.shape[1]
    heads = heads_a + heads_b
    width_a = small_heads.shape[1]
    width_b = large_heads.shape[1]
    width = width_a + width_b
    everything = width + key_rows.shape[1] + query_rows.shape[1]
    sizes = ((heads_a, width_a // heads_a), (heads_b, width_b // heads_b), state_len)
    steps = jnp.pad(
        jnp.concatenate([small_step, large_step], axis=1), ((0, 0), (0, SLOTS - heads))
    )
    steps_across = steps.T
    decay = jnp.pad(jnp.concatenate([small_decay, large_decay]), (0, SLOTS - heads))
    taps = jnp.concatenate(
        [
            small_taps,
            large_taps,
            key_taps.reshape(halo_rows + 1, -1),
            query_taps.reshape(halo_rows + 1, -1),
        ],
        axis=1,
    ).astype(F32)
    gain = jnp.concatenate([small_gain, large_gain]).astype(F32)[None]
    blocks = length // BLOCK

    def rows(columns):
        return pl.BlockSpec((BLOCK, columns), lambda i, *_: (i, 0))

    def whole(*shape):
        return pl.BlockSpec(shape, lambda i, *_: (0,) * len(shape))

    conv, packed = pl.pallas_call(
        functools.partial(conv_kernel, sizes),
        grid=(blocks,),
        in_specs=[
            rows(width_a),
            rows(width_b),
            rows(key_rows.shape[1]),
            rows(query_rows.shape[1]),
            whole(HALO, everything),
            whole(halo_rows + 1, everything),
            rows(SLOTS),
            whole(1, SLOTS),
        ],
        out_specs=[rows(everything), whole(state_len + TAIL, width)],
        out_shape=[
            jax.ShapeDtypeStruct((length, everything), BF16),
            jax.ShapeDtypeStruct((state_len + TAIL, width), BF16),
        ],
        scratch_shapes=[
            pltpu.VMEM((HALO, everything), BF16),
            pltpu.VMEM((state_len, width), F32),
            pltpu.VMEM((1, SLOTS), F32),
        ],
        cost_estimate=pl.CostEstimate(
            flops=10_000_000_000, bytes_accessed=length * everything * 4, transcendentals=0
        ),
        name="convolve",
    )(small_heads, large_heads, key_rows, query_rows, halo, taps, steps, decay[None])

    def opened(array):
        whole_log = array[state_len : state_len + 1].astype(F32)
        whole_log = whole_log + array[state_len + 1 : state_len + 2].astype(F32)
        return array[:state_len].astype(F32), whole_log

    count = lax.axis_size(SEQ)
    near = 1
    while near * near < count:
        near *= 2
    received = [opened(earlier(packed, SEQ, d)) for d in range(1, near + 1)]
    entering, log = received[-1]
    for nearer, nearer_log in received[-2::-1]:
        entering = entering * jnp.exp(nearer_log) + nearer
        log = log + nearer_log
    distance = near
    while distance < count:
        high = lax.reduce_precision(log, 8, 7)
        sent = jnp.concatenate(
            [
                entering.astype(BF16),
                high.astype(BF16),
                (log - high).astype(BF16),
            ],
            axis=0,
        )
        far_state, far_log = opened(earlier(sent, SEQ, distance))
        entering = far_state * jnp.exp(log) + entering
        log = log + far_log
        distance *= 2

    share_count = lax.axis_size("tp")
    me = lax.axis_index("tp")
    share = length // share_count
    per_share = share // BLOCK

    def out_place(i, place):
        return (reversed_bits((i // per_share) ^ place[0], share_count), i % per_share, 0)

    partial_value = pl.pallas_call(
        functools.partial(mix_kernel, sizes),
        grid_spec=pltpu.PrefetchScalarGridSpec(
            num_scalar_prefetch=1,
            grid=(blocks,),
            in_specs=[
                rows(everything),
                rows(width_a),
                rows(width_b),
                rows(SLOTS),
                pl.BlockSpec((SLOTS, BLOCK), lambda i, *_: (0, i)),
                whole(1, SLOTS),
                whole(SLOTS, 1),
                whole(1, width),
                whole(width_a, features),
                whole(width_b, features),
                whole(state_len, width),
            ],
            out_specs=pl.BlockSpec((1, BLOCK, features), out_place),
            scratch_shapes=[pltpu.VMEM((state_len, width), F32)],
        ),
        out_shape=jax.ShapeDtypeStruct((share_count, share, features), BF16),
        cost_estimate=pl.CostEstimate(
            flops=10_000_000_000, bytes_accessed=length * features * 4, transcendentals=0
        ),
        name="mix",
    )(
        jnp.reshape(me, (1,)).astype(jnp.int32),
        conv,
        small_gate,
        large_gate,
        steps,
        steps_across,
        decay[None],
        decay[:, None],
        gain,
        small_out,
        large_out,
        entering,
    )
    mix = scattered(partial_value, "tp")
    own = lax.dynamic_slice_in_dim(residual, me * share, share, 0).astype(F32)
    mixed = own + unit_rms(mix) * mixer_gain.astype(F32)
    normed_own = unit_rms(mixed) * ffn_in_gain.astype(F32)
    cut = normed_own.astype(BF16).reshape(share, -1, 2, own_rows)
    first, second = cut[:, :, 0], cut[:, :, 1]
    normed_own = jnp.stack(
        [jnp.where(side == 0, first, second), jnp.where(side == 0, second, first)], axis=1
    ).reshape(share, features)
    normed_in = collected(normed_own, "tp").reshape(length, features)
    half = features // 2
    mine, theirs = normed_in[:, :half], normed_in[:, half:]
    gate = jnp.dot(mine, gate_mine, preferred_element_type=F32)
    up_values = jnp.dot(mine, up_mine, preferred_element_type=F32)
    gate = gate + jnp.dot(theirs, gate_theirs, preferred_element_type=F32)
    up_values = up_values + jnp.dot(theirs, up_theirs, preferred_element_type=F32)
    hidden = (jax.nn.silu(gate) * up_values).astype(BF16)
    sums = []
    for down in down_parts:
        parts = lax.dot_general(
            hidden, down, (((1,), (1,)), ((), ())), preferred_element_type=F32
        ).astype(BF16)
        sums.append(scattered(parts.reshape(share_count, share, -1), "tp"))
    squares = sum(jnp.sum(part * part, axis=-1, keepdims=True) for part in sums)
    ffn_scale = 0.5 * lax.rsqrt(squares * (1.0 / features) + EPS)
    ffn = jnp.stack([part.reshape(share, -1, piece) for part in sums], axis=2)
    ffn = ffn.reshape(share, features)
    updated = mixed + ffn * ffn_scale * ffn_out_gain.astype(F32)
    return updated.astype(BF16)


def solution(mesh):
    placed = (
        P(SEQ, None),
        P(SEQ, "tp"),
        P(SEQ, "tp"),
        P(SEQ, "tp", None),
        P(SEQ, "tp", None),
        P(SEQ, "tp"),
        P(SEQ, "tp"),
        P(SEQ, "tp"),
        P(SEQ, "tp"),
        P(None, "tp"),
        P(None, "tp"),
        P(None, "tp", None),
        P(None, "tp", None),
        P("tp"),
        P("tp"),
        P("tp"),
        P("tp"),
        P("tp", None),
        P("tp", None),
        P(),
        P(),
        P(SEQ, "tp"),
        P(SEQ, "tp"),
        P(SEQ, "tp"),
        P(),
    )
    inner = 2
    outer = mesh.shape["sp"] // inner
    cut = jax.sharding.Mesh(
        mesh.devices.reshape(outer, inner, mesh.shape["tp"]), (OUTER, INNER, "tp")
    )
    return jax.shard_map(
        layer, mesh=cut, in_specs=placed, out_specs=P((*SEQ, "tp"), None), check_vma=False
    )
```

profile of v0, /device:TPU:0, one launch (start us, length us, event | category | flops | bytes accessed | tf_op | source)
XLA Modules:
  0.0 389.7 jit_solution(15312795141412024524)
XLA Ops:
  6.5 0.7 all-gather.5.cloned.1.call-update
  7.3 0.7 slice.119
  8.0 0.7 slice.120
  8.7 0.7 slice_bitcast_fusion
  10.1 4.9 %collective-permute-start = (bf16[3,1024]{1,0:T(4,128)(2,1)S(1)}, bf16[3,1024]{1,0:T(4,128)(2,1)S(1)}, u32[]{:S(2)}, u32[]{:S(2)}) collective-permute-start(bf16[3,1024]{1,0:T(4,128)(2,1)S(1)} %pad_maximum_fusion.5), channel_id=1, source_target_pairs={{0,4},{4,8},{8,12},{12,16},{16,20},{20,24},{24,28},{1,5},{5,9},{9,... | collective-permute-start | bytes 18440 | tf_op jit(solution)/shard_map/ppermute | solution.py:27
  15.0 0.7 copy_bitcast_fusion.2
  15.7 1.3 maximum_convert_fusion.taps
  17.0 1.3 fusion.24
  18.3 2.4 copy_bitcast_fusion
  21.4 1.0 copy.39.steps
  23.0 10.8 %convolve.1 = (bf16[1024,1024]{1,0:T(8,128)(2,1)}, bf16[144,512]{1,0:T(8,128)(2,1)}) custom-call(bf16[1024,256]{1,0:T(8,128)(2,1)} %small.1, bf16[1024,256]{1,0:T(8,128)(2,1)} %large.1, bf16[1024,256]{1,0:T(8,128)(2,1)} %get-tuple-element.37.keys, bf16[1024,256]{1,0:T(8,128)(2,1)} %get-tuple-element.36.queries, bf16[16,1024]{1,0:T(8,128)(2,1)} %pad.12.halo, ...), custom_call_target="tpu_custom_call" | custom-call | flops 10000000000 | bytes 4194304 | tf_op jit(solution)/shard_map/convolve/pallas_call | solution.py:358
  33.8 4.5 %collective-permute-start.1 = (bf16[144,512]{1,0:T(8,128)(2,1)}, bf16[144,512]{1,0:T(8,128)(2,1)S(1)}, u32[]{:S(2)}, u32[]{:S(2)}) collective-permute-start(bf16[144,512]{1,0:T(8,128)(2,1)} %get-tuple-element.8), channel_id=1, source_target_pairs={{0,16},{4,20},{8,24},{12,28},{1,17},{5,21},{9,25},{13,29},{2,18},{... | collective-permute-start | bytes 442376 | tf_op jit(solution)/shard_map/ppermute | solution.py:27
  38.3 2.3 collective-permute-start.2
  40.5 2.5 collective-permute-start.3
  43.1 3.4 collective-permute-start.4
  46.5 5.7 %collective-permute-done.2 = bf16[144,512]{1,0:T(8,128)(2,1)S(1)} collective-permute-done((bf16[144,512]{1,0:T(8,128)(2,1)}, bf16[144,512]{1,0:T(8,128)(2,1)S(1)}, u32[]{:S(2)}, u32[]{:S(2)}) %collective-permute-start.2) | collective-permute-done | bytes 147488 | tf_op jit(solution)/shard_map/ppermute | solution.py:27
  52.3 5.9 %collective-permute-done.3 = bf16[144,512]{1,0:T(8,128)(2,1)S(1)} collective-permute-done((bf16[144,512]{1,0:T(8,128)(2,1)}, bf16[144,512]{1,0:T(8,128)(2,1)S(1)}, u32[]{:S(2)}, u32[]{:S(2)}) %collective-permute-start.3) | collective-permute-done | bytes 147488 | tf_op jit(solution)/shard_map/ppermute | solution.py:27
  58.3 34.2 %collective-permute-start.5 = (bf16[130,512]{1,0:T(8,128)(2,1)S(1)}, bf16[130,512]{1,0:T(8,128)(2,1)S(1)}, u32[]{:S(2)}, u32[]{:S(2)}) collective-permute-start(bf16[130,512]{1,0:T(8,128)(2,1)S(1)} %pad_maximum_fusion.4), channel_id=1, source_target_pairs={{0,16},{4,20},{8,24},{12,28},{1,17},{5,21},{9,25},{13,29},{2,18},{... | collective-permute-start | bytes 399368 | tf_op jit(solution)/shard_map/ppermute | solution.py:27
  93.9 1.8 collective-permute-done.5
  95.7 0.8 multiply_add_fusion.entering
  96.5 14.4 %mix.1 = bf16[4,256,2048]{2,1,0:T(8,128)(2,1)} custom-call(s32[1]{0:T(128)} %bitcast.place, bf16[1024,1024]{1,0:T(8,128)(2,1)} %get-tuple-element.7.conv, bf16[1024,256]{1,0:T(8,128)(2,1)} %small_gate.1, bf16[1024,256]{1,0:T(8,128)(2,1)} %large_gate.1, f32[1024,8]{1,0:T(8,128)} %copy.39.steps, f32[8,1024]{1,0:T(8,128)} %get-tuple-element.28.steps_across, ...), custom_call_target="tpu_custom_call" | custom-call | flops 10000000000 | bytes 8388608 | tf_op jit(solution)/shard_map/mix/pallas_call | solution.py:425
  111.0 1.9 slice.172
  113.0 4.1 %collective-permute-done.6 = bf16[2,256,2048]{2,1,0:T(8,128)(2,1)S(1)} collective-permute-done((bf16[2,256,2048]{2,1,0:T(8,128)(2,1)S(1)}, bf16[2,256,2048]{2,1,0:T(8,128)(2,1)S(1)}, u32[]{:S(2)}, u32[]{:S(2)}) %collective-permute-start.6) | collective-permute-done | bytes 2097184 | tf_op jit(solution)/shard_map/ppermute | solution.py:27
  117.1 0.9 add_convert_fusion
  118.0 1.0 slice.174
  119.1 1.5 collective-permute-start.7
  120.6 11.2 %collective-permute-done.12 = bf16[256,1408]{1,0:T(8,128)(2,1)} collective-permute-done((bf16[256,1408]{1,0:T(8,128)(2,1)}, bf16[256,1408]{1,0:T(8,128)(2,1)}, u32[]{:S(2)}, u32[]{:S(2)}) %collective-permute-start.12) | collective-permute-done | bytes 720928 | tf_op jit(solution)/shard_map/ppermute | solution.py:27
  131.8 2.1 maximum_select_fusion
  133.9 1.2 fusion.30
  135.3 9.1 %collective-permute-done.7 = bf16[1,256,2048]{2,1,0:T(8,128)(2,1)S(1)} collective-permute-done((bf16[1,256,2048]{2,1,0:T(8,128)(2,1)}, bf16[1,256,2048]{2,1,0:T(8,128)(2,1)S(1)}, u32[]{:S(2)}, u32[]{:S(2)}) %collective-permute-start.7) | collective-permute-done | bytes 1048608 | tf_op jit(solution)/shard_map/ppermute | solution.py:27
  144.9 1.9 multiply_reduce_fusion
  146.8 2.9 multiply_convert_fusion.1
  149.8 2.6 reshape.149
  152.4 3.4 fusion.31
  156.1 1.1 pad_maximum_fusion.3
  157.2 2.3 copy.44
  159.5 1.5 collective-permute-start.8
  160.9 23.2 %collective-permute-done.8 = bf16[1,256,2048]{1,2,0:T(8,128)(2,1)S(1)} collective-permute-done((bf16[1,256,2048]{1,2,0:T(8,128)(2,1)}, bf16[1,256,2048]{1,2,0:T(8,128)(2,1)S(1)}, u32[]{:S(2)}, u32[]{:S(2)}) %collective-permute-start.8) | collective-permute-done | bytes 1048608 | tf_op jit(solution)/shard_map/ppermute | solution.py:27
  184.1 3.2 pad_maximum_fusion.1
  187.4 2.0 collective-permute-start.11
  189.5 2.4 collective-permute-done.9
  191.8 3.7 pad_maximum_fusion
  195.6 6.4 %copy.45 = bf16[4,256,2048]{2,1,0:T(8,128)(2,1)} copy(bf16[4,256,2048]{1,2,0:T(8,128)(2,1)} %pad_maximum_fusion) | data formatting | bytes 8388608 | tf_op jit(solution)/shard_map/concatenate | solution.py:268
  202.0 6.0 %fusion.10 = f32[1024,1408]{1,0:T(8,128)S(1)} fusion(bf16[1024,1408]{1,0:T(8,128)(2,1)} %all-gather.5.cloned.1.call-done, bf16[1024,2048]{1,0:T(8,128)(2,1)} %bitcast.73), kind=kOutput, calls=%fused_computation.25 | convolution fusion | flops 2952790016 | bytes 10747904 | tf_op jit(solution)/shard_map/dot_general | solution.py:477
  208.0 3.4 fusion.8
  211.4 41.7 %collective-permute-done.10 = bf16[1024,1408]{1,0:T(8,128)(2,1)} collective-permute-done((bf16[1024,1408]{1,0:T(8,128)(2,1)}, bf16[1024,1408]{1,0:T(8,128)(2,1)}, u32[]{:S(2)}, u32[]{:S(2)}) %collective-permute-start.10) | collective-permute-done | bytes 2883616 | tf_op jit(solution)/shard_map/ppermute | solution.py:27
  253.1 7.0 %fusion.6 = f32[1024,1408]{1,0:T(8,128)} fusion(bf16[1024,1408]{1,0:T(8,128)(2,1)} %collective-permute-done.10, bf16[1024,2048]{1,0:T(8,128)(2,1)S(1)} %bitcast.75), kind=kOutput, calls=%fused_computation.21 | convolution fusion | flops 2952790016 | bytes 10747904 | tf_op jit(solution)/shard_map/dot_general | solution.py:479
  260.1 54.2 %collective-permute-done.11 = bf16[1024,1408]{1,0:T(8,128)(2,1)} collective-permute-done((bf16[1024,1408]{1,0:T(8,128)(2,1)}, bf16[1024,1408]{1,0:T(8,128)(2,1)}, u32[]{:S(2)}, u32[]{:S(2)}) %collective-permute-start.11) | collective-permute-done | bytes 2883616 | tf_op jit(solution)/shard_map/ppermute | solution.py:27
  314.3 8.2 %multiply_convert_fusion = bf16[1024,1408]{1,0:T(8,128)(2,1)} fusion(f32[1024,1408]{1,0:T(8,128)S(1)} %fusion.8, f32[1024,1408]{1,0:T(8,128)S(1)} %fusion.10, f32[1024,1408]{1,0:T(8,128)} %fusion.6, bf16[1024,1408]{1,0:T(8,128)(2,1)} %collective-permute-done.11, bf16[1024,2048]{1,0:T(8,128)(2,1)S(1)} %bitcast.76), kind=kOutput, calls=%fused_computation | convolution fusion | flops 2964324352 | bytes 25165824 | tf_op jit(solution)/shard_map/dot_general | solution.py:480
  322.6 6.1 %convolution_convert_fusion.1 = bf16[1024,1024]{1,0:T(8,128)(2,1)S(1)} fusion(bf16[1024,1408]{1,0:T(8,128)(2,1)} %multiply_convert_fusion, bf16[1024,1408]{1,0:T(8,128)(2,1)} %all-gather.9.cloned.1.call-done), kind=kOutput, calls=%fused_computation.19 | convolution fusion | flops 2953838592 | bytes 7864320 | tf_op jit(solution)/shard_map/dot_general | solution.py:484
  328.7 1.5 fusion.28
  330.2 6.1 %convolution_convert_fusion = bf16[1024,1024]{1,0:T(8,128)(2,1)S(1)} fusion(bf16[1024,1408]{1,0:T(8,128)(2,1)} %multiply_convert_fusion, bf16[1024,1408]{1,0:T(8,128)(2,1)} %all-gather.11.cloned.1.call-done), kind=kOutput, calls=%fused_computation.18 | convolution fusion | flops 2953838592 | bytes 7864320 | tf_op jit(solution)/shard_map/dot_general | solution.py:484
  337.6 1.6 fusion.1
  339.3 1.5 collective-permute-start.14
  341.2 0.9 slice.188
  342.7 11.4 %collective-permute-done.14 = bf16[1,256,1024]{2,1,0:T(8,128)(2,1)S(1)} collective-permute-done((bf16[1,256,1024]{2,1,0:T(8,128)(2,1)S(1)}, bf16[1,256,1024]{2,1,0:T(8,128)(2,1)S(1)}, u32[]{:S(2)}, u32[]{:S(2)}) %collective-permute-start.14) | collective-permute-done | bytes 524320 | tf_op jit(solution)/shard_map/ppermute | solution.py:27
  354.1 1.2 multiply_reduce_fusion.2
  355.3 3.5 stack_reshape_squeeze.6
  358.7 6.3 %collective-permute-done.16 = bf16[1,256,1024]{2,1,0:T(8,128)(2,1)} collective-permute-done((bf16[1,256,1024]{2,1,0:T(8,128)(2,1)}, bf16[1,256,1024]{2,1,0:T(8,128)(2,1)}, u32[]{:S(2)}, u32[]{:S(2)}) %collective-permute-start.16) | collective-permute-done | bytes 524320 | tf_op jit(solution)/shard_map/ppermute | solution.py:27
  365.0 2.4 multiply_reduce_fusion.1
  367.4 3.4 stack_reshape_squeeze.7
  370.8 4.8 %pad_maximum_fusion.2 = f32[256,8,2,128]{3,2,1,0:T(2,128)} fusion(f32[256,8,1,128]{3,2,1,0:T(1,128)} %stack_reshape_squeeze.7, f32[256,8,1,128]{3,2,1,0:T(1,128)} %stack_reshape_squeeze.6), kind=kLoop, calls=%fused_computation.4 | loop fusion | flops 524288 | bytes 4194304 | tf_op jit(solution)/shard_map/stack | solution.py:490
  375.6 3.9 reshape.153
  379.5 3.6 add_convert_fusion.1
  (74 shorter events, 7.0 us)
Async XLA Ops:
  6.5 14.2 %copy-start.10 = (f32[4]{0:T(128)S(1)}, f32[4]{0:T(128)}, u32[]{:S(2)}) copy-start(f32[4]{0:T(128)} %param.38) | copy-start | bytes 52
  6.5 14.2 %copy-start.9 = (f32[2]{0:T(128)S(1)}, f32[2]{0:T(128)}, u32[]{:S(2)}) copy-start(f32[2]{0:T(128)} %param.39) | copy-start | bytes 28
  6.5 180.8 %all-gather.5.cloned.1.call-start = ((), (), s32[]{:S(2)}) async-start(), calls=%async_computation | async-start | bytes 3604480 | tf_op jit(solution)/shard_map/all_gather | solution.py:316
  7.3 180.2 %all-gather.7.cloned.1.call-start = ((), (), s32[]{:S(2)}) async-start(), calls=%async_computation.1 | async-start | bytes 3604480 | tf_op jit(solution)/shard_map/all_gather | solution.py:317
  10.1 12.3 %collective-permute-start = (bf16[3,1024]{1,0:T(4,128)(2,1)S(1)}, bf16[3,1024]{1,0:T(4,128)(2,1)S(1)}, u32[]{:S(2)}, u32[]{:S(2)}) collective-permute-start(bf16[3,1024]{1,0:T(4,128)(2,1)S(1)} %pad_maximum_fusion.5), channel_id=1, source_target_pairs={{0,4},{4,8},{8,12},{12,16},{16,20},{20,24},{24,28},{1,5},{5,9},{9,... | collective-permute-start | bytes 18440 | tf_op jit(solution)/shard_map/ppermute | solution.py:27
  23.0 70.3 %copy-start.11 = (bf16[256]{0:T(256)(128)(2,1)S(1)}, bf16[256]{0:T(256)(128)(2,1)}, u32[]{:S(2)}) copy-start(bf16[256]{0:T(256)(128)(2,1)} %param.40) | copy-start | bytes 1540
  23.0 70.3 %copy-start.12 = (bf16[256]{0:T(256)(128)(2,1)S(1)}, bf16[256]{0:T(256)(128)(2,1)}, u32[]{:S(2)}) copy-start(bf16[256]{0:T(256)(128)(2,1)} %param.41) | copy-start | bytes 1540
  33.8 12.7 %collective-permute-start.1 = (bf16[144,512]{1,0:T(8,128)(2,1)}, bf16[144,512]{1,0:T(8,128)(2,1)S(1)}, u32[]{:S(2)}, u32[]{:S(2)}) collective-permute-start(bf16[144,512]{1,0:T(8,128)(2,1)} %get-tuple-element.8), channel_id=1, source_target_pairs={{0,16},{4,20},{8,24},{12,28},{1,17},{5,21},{9,25},{13,29},{2,18},{... | collective-permute-start | bytes 442376 | tf_op jit(solution)/shard_map/ppermute | solution.py:27
  38.3 14.0 %collective-permute-start.2 = (bf16[144,512]{1,0:T(8,128)(2,1)}, bf16[144,512]{1,0:T(8,128)(2,1)S(1)}, u32[]{:S(2)}, u32[]{:S(2)}) collective-permute-start(bf16[144,512]{1,0:T(8,128)(2,1)} %get-tuple-element.8), channel_id=1, source_target_pairs={{0,12},{4,16},{8,20},{12,24},{16,28},{1,13},{5,17},{9,21},{13,25},... | collective-permute-start | bytes 442376 | tf_op jit(solution)/shard_map/ppermute | solution.py:27
  40.5 17.6 %collective-permute-start.3 = (bf16[144,512]{1,0:T(8,128)(2,1)}, bf16[144,512]{1,0:T(8,128)(2,1)S(1)}, u32[]{:S(2)}, u32[]{:S(2)}) collective-permute-start(bf16[144,512]{1,0:T(8,128)(2,1)} %get-tuple-element.8), channel_id=1, source_target_pairs={{0,8},{4,12},{8,16},{12,20},{16,24},{20,28},{1,9},{5,13},{9,17},{1... | collective-permute-start | bytes 442376 | tf_op jit(solution)/shard_map/ppermute | solution.py:27
  43.1 15.1 %collective-permute-start.4 = (bf16[144,512]{1,0:T(8,128)(2,1)}, bf16[144,512]{1,0:T(8,128)(2,1)S(1)}, u32[]{:S(2)}, u32[]{:S(2)}) collective-permute-start(bf16[144,512]{1,0:T(8,128)(2,1)} %get-tuple-element.8), channel_id=1, source_target_pairs={{0,4},{4,8},{8,12},{12,16},{16,20},{20,24},{24,28},{1,5},{5,9},{9,... | collective-permute-start | bytes 442376 | tf_op jit(solution)/shard_map/ppermute | solution.py:27
  46.5 276.1 %all-gather.9.cloned.1.call-start = ((), (), s32[]{:S(2)}) async-start(), calls=%async_computation.2 | async-start | bytes 3604480 | tf_op jit(solution)/shard_map/all_gather | solution.py:323
  58.3 37.4 %collective-permute-start.5 = (bf16[130,512]{1,0:T(8,128)(2,1)S(1)}, bf16[130,512]{1,0:T(8,128)(2,1)S(1)}, u32[]{:S(2)}, u32[]{:S(2)}) collective-permute-start(bf16[130,512]{1,0:T(8,128)(2,1)S(1)} %pad_maximum_fusion.4), channel_id=1, source_target_pairs={{0,16},{4,20},{8,24},{12,28},{1,17},{5,21},{9,25},{13,29},{2,18},{... | collective-permute-start | bytes 399368 | tf_op jit(solution)/shard_map/ppermute | solution.py:27
  111.0 6.1 %copy-start = (bf16[4,256,2048]{2,1,0:T(8,128)(2,1)S(1)}, bf16[4,256,2048]{2,1,0:T(8,128)(2,1)}, u32[]{:S(2)}) copy-start(bf16[4,256,2048]{2,1,0:T(8,128)(2,1)} %mix.1) | copy-start | bytes 12582916
  112.9 4.2 %collective-permute-start.6 = (bf16[2,256,2048]{2,1,0:T(8,128)(2,1)S(1)}, bf16[2,256,2048]{2,1,0:T(8,128)(2,1)S(1)}, u32[]{:S(2)}, u32[]{:S(2)}) collective-permute-start(bf16[2,256,2048]{2,1,0:T(8,128)(2,1)S(1)} %slice.172), channel_id=1, source_target_pairs={{0,1},{1,0},{2,3},{3,2},{4,5},{5,4},{6,7},{7,6},{8,9},{9,8},{10,11... | collective-permute-start | bytes 6291464 | tf_op jit(solution)/shard_map/ppermute | solution.py:27
  112.9 18.9 %collective-permute-start.12 = (bf16[256,1408]{1,0:T(8,128)(2,1)}, bf16[256,1408]{1,0:T(8,128)(2,1)}, u32[]{:S(2)}, u32[]{:S(2)}) collective-permute-start(bf16[256,1408]{1,0:T(8,128)(2,1)} %param.48), channel_id=1, source_target_pairs={{0,4},{4,0},{1,5},{5,1},{2,6},{6,2},{3,7},{7,3},{8,12},{12,8},{9,1... | collective-permute-start | bytes 2162696 | tf_op jit(solution)/shard_map/ppermute | solution.py:27
  118.0 2.5 copy-start.5
  118.0 2.5 copy-start.6
  119.1 25.4 %collective-permute-start.7 = (bf16[1,256,2048]{2,1,0:T(8,128)(2,1)}, bf16[1,256,2048]{2,1,0:T(8,128)(2,1)S(1)}, u32[]{:S(2)}, u32[]{:S(2)}) collective-permute-start(bf16[1,256,2048]{2,1,0:T(8,128)(2,1)} %slice.174), channel_id=1, source_target_pairs={{0,2},{1,3},{2,0},{3,1},{4,6},{5,7},{6,4},{7,5},{8,10},{9,11},{10,... | collective-permute-start | bytes 3145736 | tf_op jit(solution)/shard_map/ppermute | solution.py:27
  135.1 195.1 %all-gather.11.cloned.1.call-start = ((), (), s32[]{:S(2)}) async-start(), calls=%async_computation.3 | async-start | bytes 3604480 | tf_op jit(solution)/shard_map/all_gather | solution.py:323
  159.5 24.7 %collective-permute-start.8 = (bf16[1,256,2048]{1,2,0:T(8,128)(2,1)}, bf16[1,256,2048]{1,2,0:T(8,128)(2,1)S(1)}, u32[]{:S(2)}, u32[]{:S(2)}) collective-permute-start(bf16[1,256,2048]{1,2,0:T(8,128)(2,1)} %bitcast.70), channel_id=1, source_target_pairs={{0,2},{1,3},{2,0},{3,1},{4,6},{5,7},{6,4},{7,5},{8,10},{9,11},{10,... | collective-permute-start | bytes 3145736 | tf_op jit(solution)/shard_map/ppermute | solution.py:27
  184.1 3.2 copy-start.4
  187.3 4.5 %collective-permute-start.9 = (bf16[2,256,2048]{1,2,0:T(8,128)(2,1)}, bf16[2,256,2048]{1,2,0:T(8,128)(2,1)}, u32[]{:S(2)}, u32[]{:S(2)}) collective-permute-start(bf16[2,256,2048]{1,2,0:T(8,128)(2,1)} %pad_maximum_fusion.1), channel_id=1, source_target_pairs={{0,1},{1,0},{2,3},{3,2},{4,5},{5,4},{6,7},{7,6},{8,9},{9,8},{10,11... | collective-permute-start | bytes 6291464 | tf_op jit(solution)/shard_map/ppermute | solution.py:27
  187.3 65.7 %collective-permute-start.10 = (bf16[1024,1408]{1,0:T(8,128)(2,1)}, bf16[1024,1408]{1,0:T(8,128)(2,1)}, u32[]{:S(2)}, u32[]{:S(2)}) collective-permute-start(bf16[1024,1408]{1,0:T(8,128)(2,1)} %all-gather.5.cloned.1.call-done), channel_id=1, source_target_pairs={{0,4},{4,0},{1,5},{5,1},{2,6},{6,2},{3,7},{7,3},{8,12},{12,8},{9,1... | collective-permute-start | bytes 8650760 | tf_op jit(solution)/shard_map/ppermute | solution.py:27
  187.4 126.9 %collective-permute-start.11 = (bf16[1024,1408]{1,0:T(8,128)(2,1)}, bf16[1024,1408]{1,0:T(8,128)(2,1)}, u32[]{:S(2)}, u32[]{:S(2)}) collective-permute-start(bf16[1024,1408]{1,0:T(8,128)(2,1)} %all-gather.7.cloned.1.call-done), channel_id=1, source_target_pairs={{0,4},{4,0},{1,5},{5,1},{2,6},{6,2},{3,7},{7,3},{8,12},{12,8},{9,1... | collective-permute-start | bytes 8650760 | tf_op jit(solution)/shard_map/ppermute | solution.py:27
  202.0 6.0 %copy-start.2 = (bf16[4,256,2048]{2,1,0:T(8,128)(2,1)S(1)}, bf16[4,256,2048]{2,1,0:T(8,128)(2,1)}, u32[]{:S(2)}) copy-start(bf16[4,256,2048]{2,1,0:T(8,128)(2,1)} %copy.45) | copy-start | bytes 12582916
  202.0 6.0 %copy-start.8 = (bf16[1024,1408]{1,0:T(8,128)(2,1)S(1)}, bf16[1024,1408]{1,0:T(8,128)(2,1)}, u32[]{:S(2)}) copy-start(bf16[1024,1408]{1,0:T(8,128)(2,1)} %all-gather.7.cloned.1.call-done) | copy-start | bytes 8650756
  330.2 6.9 %collective-permute-start.13 = (bf16[2,256,1024]{2,1,0:T(8,128)(2,1)}, bf16[2,256,1024]{2,1,0:T(8,128)(2,1)}, u32[]{:S(2)}, u32[]{:S(2)}) collective-permute-start(bf16[2,256,1024]{2,1,0:T(8,128)(2,1)} %bitcast.17), channel_id=1, source_target_pairs={{0,1},{1,0},{2,3},{3,2},{4,5},{5,4},{6,7},{7,6},{8,9},{9,8},{10,11... | collective-permute-start | bytes 3145736 | tf_op jit(solution)/shard_map/ppermute | solution.py:27
  336.4 1.2 copy-start.3
  336.5 4.3 %collective-permute-start.15 = (bf16[2,256,1024]{2,1,0:T(8,128)(2,1)S(1)}, bf16[2,256,1024]{2,1,0:T(8,128)(2,1)S(1)}, u32[]{:S(2)}, u32[]{:S(2)}) collective-permute-start(bf16[2,256,1024]{2,1,0:T(8,128)(2,1)S(1)} %bitcast.81), channel_id=1, source_target_pairs={{0,1},{1,0},{2,3},{3,2},{4,5},{5,4},{6,7},{7,6},{8,9},{9,8},{10,11... | collective-permute-start | bytes 3145736 | tf_op jit(solution)/shard_map/ppermute | solution.py:27
  339.3 14.9 %collective-permute-start.14 = (bf16[1,256,1024]{2,1,0:T(8,128)(2,1)S(1)}, bf16[1,256,1024]{2,1,0:T(8,128)(2,1)S(1)}, u32[]{:S(2)}, u32[]{:S(2)}) collective-permute-start(bf16[1,256,1024]{2,1,0:T(8,128)(2,1)S(1)} %slice.183), channel_id=1, source_target_pairs={{0,2},{1,3},{2,0},{3,1},{4,6},{5,7},{6,4},{7,5},{8,10},{9,11},{10,... | collective-permute-start | bytes 1572872 | tf_op jit(solution)/shard_map/ppermute | solution.py:27
  340.8 1.9 copy-start.7
  341.2 14.0 %copy-start.1 = (bf16[2,256,1024]{2,1,0:T(8,128)(2,1)}, bf16[2,256,1024]{2,1,0:T(8,128)(2,1)S(1)}, u32[]{:S(2)}) copy-start(bf16[2,256,1024]{2,1,0:T(8,128)(2,1)S(1)} %fusion) | copy-start | bytes 3145732
  342.1 22.9 %collective-permute-start.16 = (bf16[1,256,1024]{2,1,0:T(8,128)(2,1)}, bf16[1,256,1024]{2,1,0:T(8,128)(2,1)}, u32[]{:S(2)}, u32[]{:S(2)}) collective-permute-start(bf16[1,256,1024]{2,1,0:T(8,128)(2,1)} %slice.188), channel_id=1, source_target_pairs={{0,2},{1,3},{2,0},{3,1},{4,6},{5,7},{6,4},{7,5},{8,10},{9,11},{10,... | collective-permute-start | bytes 1572872 | tf_op jit(solution)/shard_map/ppermute | solution.py:27
Sparse Core Ops, SparseCore 0:
  8.9 67.4 all-gather.4
  78.0 73.9 all-gather.6
  153.6 57.7 all-gather.8
  212.8 57.7 all-gather.10
where the time goes:
time: 391 us; the launch traced here: 390 us
  waiting for transfers between devices  178 us (46%)
  starting transfers between devices  59.8 us (15%)
  local copies, waits for them, and re-layouts  40.9 us (10%)
  matrix products  36.9 us (9%)
  other arithmetic  35.5 us (9%)
  Pallas kernels  25.2 us (6%)
  between operations  13.4 us (3%)
    ppermute x17, waiting for transfers between devices, moved(): return lax.ppermute(block, axis, route)  177 us
    ppermute x17, starting transfers between devices, moved(): return lax.ppermute(block, axis, route)  59.5 us
    pallas_call x1, Pallas kernels, layer(): pl.pallas_call(functools.partial(mix_kernel, sizes), grid_spec=pltpu.Pref...  14.4 us
    dot_general x2, matrix products, layer(): lax.dot_general(hidden, down, (((1,), (1,)), ((), ())), preferred_element...  12.2 us
    pallas_call x1, Pallas kernels, layer(): pl.pallas_call(functools.partial(conv_kernel, sizes), grid=(blocks,), in_...  10.8 us
    dot_general x1, matrix products, layer(): jnp.dot(theirs, up_theirs, preferred_element_type=F32)  8.24 us
  transfers between devices with their start and end apart: 21, of which 12 were waited for; matrix products, arithmetic and copies ran while one was open for 24% of the time, Pallas kernels for 6%

commit v1 on v0

--- a/solution.py
+++ b/solution.py
@@ -240,6 +240,44 @@
     return values * lax.rsqrt(jnp.mean(values * values, axis=-1, keepdims=True) + EPS)
 
 
+def norm_kernel(chunk, side, one, other, own, mixer_gain, ffn_gain, mixed_out, normed_out):
+    mix = one[...].astype(F32) + other[...].astype(F32)
+    mixed = own[...].astype(F32) + unit_rms(mix) * mixer_gain[...].astype(F32)
+    mixed_out[...] = mixed
+    normed = (unit_rms(mixed) * ffn_gain[...].astype(F32)).astype(BF16)
+    half = normed.shape[1] // 2
+    for j in range(half // chunk):
+        first = normed[:, 2 * j * chunk : (2 * j + 1) * chunk]
+        second = normed[:, (2 * j + 1) * chunk : (2 * j + 2) * chunk]
+        at = j * chunk
+
+        @pl.when(side[0] == 0)
+        def _():
+            normed_out[:, at : at + chunk] = first
+            normed_out[:, half + at : half + at + chunk] = second
+
+        @pl.when(side[0] != 0)
+        def _():
+            normed_out[:, at : at + chunk] = second
+            normed_out[:, half + at : half + at + chunk] = first
+
+
+def last_kernel(piece, *refs):
+    *terms, mixed, gain, out = refs
+    sums = []
+    for p in range(PARTS):
+        sums.append(terms[2 * p][...].astype(F32) + terms[2 * p + 1][...].astype(F32))
+    features = mixed.shape[1]
+    squares = sum(jnp.sum(part * part, axis=-1, keepdims=True) for part in sums)
+    scale = 0.5 * lax.rsqrt(squares * (1.0 / features) + EPS)
+    for j in range(features // piece):
+        at = j * piece
+        here = j // PARTS * piece
+        value = sums[j % PARTS][:, here : here + piece] * scale
+        value = value * gain[:, at : at + piece].astype(F32)
+        out[:, at : at + piece] = (mixed[:, at : at + piece] + value).astype(BF16)
+
+
 def reversed_bits(value, count):
     out = 0
     bit = 1
@@ -251,13 +289,13 @@
 
 def scattered(blocks, axis):
     bit = 1
-    while blocks.shape[0] > 1:
+    while True:
         half = blocks.shape[0] // 2
         other = paired(blocks[half:], axis, bit)
-        total = blocks[:half].astype(F32) + other.astype(F32)
+        if half == 1:
+            return blocks[0], other[0]
+        blocks = (blocks[:half].astype(F32) + other.astype(F32)).astype(BF16)
         bit *= 2
-        blocks = total if half == 1 else total.astype(BF16)
-    return blocks[0].astype(F32)
 
 
 def collected(block, axis):
@@ -462,15 +500,37 @@
         large_out,
         entering,
     )
-    mix = scattered(partial_value, "tp")
-    own = lax.dynamic_slice_in_dim(residual, me * share, share, 0).astype(F32)
-    mixed = own + unit_rms(mix) * mixer_gain.astype(F32)
-    normed_own = unit_rms(mixed) * ffn_in_gain.astype(F32)
-    cut = normed_own.astype(BF16).reshape(share, -1, 2, own_rows)
-    first, second = cut[:, :, 0], cut[:, :, 1]
-    normed_own = jnp.stack(
-        [jnp.where(side == 0, first, second), jnp.where(side == 0, second, first)], axis=1
-    ).reshape(share, features)
+    mix_one, mix_other = scattered(partial_value, "tp")
+    own = lax.dynamic_slice_in_dim(residual, me * share, share, 0)
+    tile = BLOCK // 2
+
+    def strips(columns):
+        return pl.BlockSpec((tile, columns), lambda i, *_: (i, 0))
+
+    mixed, normed_own = pl.pallas_call(
+        functools.partial(norm_kernel, own_rows),
+        grid_spec=pltpu.PrefetchScalarGridSpec(
+            num_scalar_prefetch=1,
+            grid=(share // tile,),
+            in_specs=[strips(features)] * 3 + [whole(1, features)] * 2,
+            out_specs=[strips(features)] * 2,
+        ),
+        out_shape=[
+            jax.ShapeDtypeStruct((share, features), F32),
+            jax.ShapeDtypeStruct((share, features), BF16),
+        ],
+        cost_estimate=pl.CostEstimate(
+            flops=1_000_000_000, bytes_accessed=share * features * 12, transcendentals=0
+        ),
+        name="norms",
+    )(
+        jnp.reshape(side, (1,)).astype(jnp.int32),
+        mix_one,
+        mix_other,
+        own,
+        mixer_gain[None],
+        ffn_in_gain[None],
+    )
     normed_in = collected(normed_own, "tp").reshape(length, features)
     half = features // 2
     mine, theirs = normed_in[:, :half], normed_in[:, half:]
@@ -484,13 +544,18 @@
         parts = lax.dot_general(
             hidden, down, (((1,), (1,)), ((), ())), preferred_element_type=F32
         ).astype(BF16)
-        sums.append(scattered(parts.reshape(share_count, share, -1), "tp"))
-    squares = sum(jnp.sum(part * part, axis=-1, keepdims=True) for part in sums)
-    ffn_scale = 0.5 * lax.rsqrt(squares * (1.0 / features) + EPS)
-    ffn = jnp.stack([part.reshape(share, -1, piece) for part in sums], axis=2)
-    ffn = ffn.reshape(share, features)
-    updated = mixed + ffn * ffn_scale * ffn_out_gain.astype(F32)
-    return updated.astype(BF16)
+        sums.extend(scattered(parts.reshape(share_count, share, -1), "tp"))
+    return pl.pallas_call(
+        functools.partial(last_kernel, piece),
+        grid=(share // tile,),
+        in_specs=[strips(features // PARTS)] * (2 * PARTS) + [strips(features), whole(1, features)],
+        out_specs=strips(features),
+        out_shape=jax.ShapeDtypeStruct((share, features), BF16),
+        cost_estimate=pl.CostEstimate(
+            flops=1_000_000_000, bytes_accessed=share * features * 10, transcendentals=0
+        ),
+        name="last",
+    )(*sums, mixed, ffn_out_gain[None])
 
 
 def solution(mesh):

time: 391 us -> 388 us (level)
  waiting for transfers between devices: 178 us -> 209 us
  other arithmetic: 35.5 us -> 13 us
  local copies, waits for them, and re-layouts: 40.9 us -> 23.5 us
  Pallas kernels: 25.2 us -> 34.5 us
    ppermute x17, waiting for transfers between devices: 177 us -> 208 us  [moved(): return lax.ppermute(block, axis, route)]
    pallas_call x0 -> x2, Pallas kernels: none -> 9.3 us  [the longest x1 4.86 us: layer(): pl.pallas_call(functools.partial(norm_kernel, own_rows), grid_spec=pltpu....]
    another operation x3 -> x0, local copies, waits for them, and re-layouts: 9.17 us -> none  [the longest x2 6.89 us: layer(): ffn = jnp.stack([part.reshape(share, -1, piece) for part in sums], axis=2)]
    reshape x2 -> x0, local copies, waits for them, and re-layouts: 6.52 us -> none  [the longest x1 3.89 us: layer(): ffn = ffn.reshape(share, features)]
    concatenate x1 -> x0, local copies, waits for them, and re-layouts: 6.39 us -> none  [collected(): blocks = jnp.concatenate([blocks, other], axis=0)]
    convert_element_type x8 -> x3, other arithmetic: 9.49 us -> 3.19 us  [scattered(): blocks = (blocks[:half].astype(F32) + other.astype(F32)).astype(BF16)]
    reduce_sum x4 -> x0, other arithmetic: 5.87 us -> none  [the longest x2 3.51 us: layer(): jnp.sum(part * part, axis=-1, keepdims=True)]
    another operation x2 -> x0, other arithmetic: 5.85 us -> none  [the longest x1 4.79 us: layer(): ffn = jnp.stack([part.reshape(share, -1, piece) for part in sums], axis=2)]
  transfers between devices with their start and end apart: 21 -> 21, of which waited for: 12 -> 11; matrix products, arithmetic and copies ran while one was open for 24% -> 17% of each run, Pallas kernels for 6% -> 8%
where the time goes in v1:
time: 388 us; the launch traced here: 387 us
  waiting for transfers between devices  209 us (54%)
  starting transfers between devices  60 us (15%)
  Pallas kernels  34.5 us (9%)
  matrix products  33.7 us (9%)
  local copies, waits for them, and re-layouts  23.5 us (6%)
  between operations  13.4 us (3%)
  other arithmetic  13 us (3%)
    ppermute x17, waiting for transfers between devices, moved(): return lax.ppermute(block, axis, route)  208 us
    ppermute x17, starting transfers between devices, moved(): return lax.ppermute(block, axis, route)  59.6 us
    pallas_call x1, Pallas kernels, layer(): pl.pallas_call(functools.partial(mix_kernel, sizes), grid_spec=pltpu.Pref...  14.4 us
    dot_general x2, matrix products, layer(): lax.dot_general(hidden, down, (((1,), (1,)), ((), ())), preferred_element...  11.8 us
    pallas_call x1, Pallas kernels, layer(): pl.pallas_call(functools.partial(conv_kernel, sizes), grid=(blocks,), in_...  10.8 us
  transfers between devices with their start and end apart: 21, of which 11 were waited for; matrix products, arithmetic and copies ran while one was open for 17% of the time, Pallas kernels for 8%

profile of v1, /device:TPU:0, one launch (start us, length us, event | category | flops | bytes accessed | tf_op | source)
XLA Modules:
  0.0 387.3 jit_solution(14576155045938493376)
XLA Ops:
  6.5 0.7 all-gather.5.cloned.1.call-update
  7.3 0.7 slice.113
  8.0 0.7 slice.114
  8.7 0.7 slice_bitcast_fusion.3
  9.4 0.7 slice_bitcast_fusion.4
  10.1 4.9 %collective-permute-start = (bf16[3,1024]{1,0:T(4,128)(2,1)S(1)}, bf16[3,1024]{1,0:T(4,128)(2,1)S(1)}, u32[]{:S(2)}, u32[]{:S(2)}) collective-permute-start(bf16[3,1024]{1,0:T(4,128)(2,1)S(1)} %pad_maximum_fusion.3), channel_id=1, source_target_pairs={{0,4},{4,8},{8,12},{12,16},{16,20},{20,24},{24,28},{1,5},{5,9},{9,... | collective-permute-start | bytes 18440 | tf_op jit(solution)/shard_map/ppermute | solution.py:27
  15.0 0.7 copy_bitcast_fusion.2
  15.7 1.3 maximum_convert_fusion.taps
  17.0 1.4 fusion.21
  18.4 2.4 copy_bitcast_fusion
  20.8 0.7 fusion.40.decay
  21.4 1.0 copy.26.steps
  22.5 0.6 pad.12.halo
  23.1 10.8 %convolve.1 = (bf16[1024,1024]{1,0:T(8,128)(2,1)}, bf16[144,512]{1,0:T(8,128)(2,1)}) custom-call(bf16[1024,256]{1,0:T(8,128)(2,1)} %small.1, bf16[1024,256]{1,0:T(8,128)(2,1)} %large.1, bf16[1024,256]{1,0:T(8,128)(2,1)} %get-tuple-element.39.keys, bf16[1024,256]{1,0:T(8,128)(2,1)} %get-tuple-element.38.queries, bf16[16,1024]{1,0:T(8,128)(2,1)} %pad.12.halo, ...), custom_call_target="tpu_custom_call" | custom-call | flops 10000000000 | bytes 4194304 | tf_op jit(solution)/shard_map/convolve/pallas_call | solution.py:396
  33.9 4.5 %collective-permute-start.1 = (bf16[144,512]{1,0:T(8,128)(2,1)}, bf16[144,512]{1,0:T(8,128)(2,1)S(1)}, u32[]{:S(2)}, u32[]{:S(2)}) collective-permute-start(bf16[144,512]{1,0:T(8,128)(2,1)} %get-tuple-element.10), channel_id=1, source_target_pairs={{0,16},{4,20},{8,24},{12,28},{1,17},{5,21},{9,25},{13,29},{2,18},{... | collective-permute-start | bytes 442376 | tf_op jit(solution)/shard_map/ppermute | solution.py:27
  38.4 2.2 collective-permute-start.2
  40.6 2.5 collective-permute-start.3
  43.2 3.4 collective-permute-start.4
  46.7 5.7 %collective-permute-done.2 = bf16[144,512]{1,0:T(8,128)(2,1)S(1)} collective-permute-done((bf16[144,512]{1,0:T(8,128)(2,1)}, bf16[144,512]{1,0:T(8,128)(2,1)S(1)}, u32[]{:S(2)}, u32[]{:S(2)}) %collective-permute-start.2) | collective-permute-done | bytes 147488 | tf_op jit(solution)/shard_map/ppermute | solution.py:27
  52.4 5.9 %collective-permute-done.3 = bf16[144,512]{1,0:T(8,128)(2,1)S(1)} collective-permute-done((bf16[144,512]{1,0:T(8,128)(2,1)}, bf16[144,512]{1,0:T(8,128)(2,1)S(1)}, u32[]{:S(2)}, u32[]{:S(2)}) %collective-permute-start.3) | collective-permute-done | bytes 147488 | tf_op jit(solution)/shard_map/ppermute | solution.py:27
  58.5 34.1 %collective-permute-start.5 = (bf16[130,512]{1,0:T(8,128)(2,1)S(1)}, bf16[130,512]{1,0:T(8,128)(2,1)S(1)}, u32[]{:S(2)}, u32[]{:S(2)}) collective-permute-start(bf16[130,512]{1,0:T(8,128)(2,1)S(1)} %pad_maximum_fusion.2), channel_id=1, source_target_pairs={{0,16},{4,20},{8,24},{12,28},{1,17},{5,21},{9,25},{13,29},{2,18},{... | collective-permute-start | bytes 399368 | tf_op jit(solution)/shard_map/ppermute | solution.py:27
  92.6 0.7 copy.28.decay_across
  93.3 0.6 maximum_convert_fusion.1.gain
  93.9 1.8 collective-permute-done.5
  95.7 0.8 multiply_add_fusion.entering
  96.5 14.4 %mix.1 = bf16[4,256,2048]{2,1,0:T(8,128)(2,1)} custom-call(s32[1]{0:T(128)} %bitcast.1.place, bf16[1024,1024]{1,0:T(8,128)(2,1)} %get-tuple-element.9.conv, bf16[1024,256]{1,0:T(8,128)(2,1)} %small_gate.1, bf16[1024,256]{1,0:T(8,128)(2,1)} %large_gate.1, f32[1024,8]{1,0:T(8,128)} %copy.26.steps, f32[8,1024]{1,0:T(8,128)} %get-tuple-element.30.steps_across, ...), custom_call_target="tpu_custom_call" | custom-call | flops 10000000000 | bytes 8388608 | tf_op jit(solution)/shard_map/mix/pallas_call | solution.py:463
  111.0 3.3 slice.164
  114.3 18.5 %collective-permute-done.12 = bf16[256,1408]{1,0:T(8,128)(2,1)S(1)} collective-permute-done((bf16[256,1408]{1,0:T(8,128)(2,1)S(1)}, bf16[256,1408]{1,0:T(8,128)(2,1)S(1)}, u32[]{:S(2)}, u32[]{:S(2)}) %collective-permute-start.12) | collective-permute-done | bytes 720928 | tf_op jit(solution)/shard_map/ppermute | solution.py:27
  133.1 2.4 add_convert_fusion
  135.5 1.2 fusion.27
  136.7 1.5 collective-permute-start.7
  138.1 1.3 fusion.28
  139.7 0.6 broadcast_in_dim.22.mixer_gain
  140.3 0.6 broadcast_in_dim.23.ffn_gain
  140.9 2.3 constant_dynamic-slice_fusion.own
  143.2 18.3 %collective-permute-done.7 = bf16[1,256,2048]{2,1,0:T(8,128)(2,1)S(1)} collective-permute-done((bf16[1,256,2048]{2,1,0:T(8,128)(2,1)S(1)}, bf16[1,256,2048]{2,1,0:T(8,128)(2,1)S(1)}, u32[]{:S(2)}, u32[]{:S(2)}) %collective-permute-start.7) | collective-permute-done | bytes 1048608 | tf_op jit(solution)/shard_map/ppermute | solution.py:27
  161.5 1.0 copy-done.9
  162.5 4.9 %norms.1 = (f32[256,2048]{1,0:T(8,128)}, bf16[256,2048]{1,0:T(8,128)(2,1)}) custom-call(s32[1]{0:T(128)} %bitcast.side, bf16[256,2048]{1,0:T(8,128)(2,1)} %get-tuple-element.20.one, bf16[256,2048]{1,0:T(8,128)(2,1)} %bitcast.89, bf16[256,2048]{1,0:T(8,128)(2,1)} %constant_dynamic-slice_fusion.own, bf16[1,2048]{1,0:T(2,128)(2,1)} %broadcast_in_dim.22.mixer_gain, ...), custom_call_target="tpu_custom_call" | custom-call | flops 1000000000 | bytes 6291456 | tf_op jit(solution)/shard_map/norms/pallas_call | solution.py:510
  167.4 1.5 collective-permute-start.8
  168.8 22.8 %collective-permute-done.8 = bf16[1,256,2048]{2,1,0:T(8,128)(2,1)S(1)} collective-permute-done((bf16[1,256,2048]{2,1,0:T(8,128)(2,1)}, bf16[1,256,2048]{2,1,0:T(8,128)(2,1)S(1)}, u32[]{:S(2)}, u32[]{:S(2)}) %collective-permute-start.8) | collective-permute-done | bytes 1048608 | tf_op jit(solution)/shard_map/ppermute | solution.py:27
  191.6 2.8 pad_maximum_fusion.1
  194.4 0.8 collective-permute-start.10
  195.3 1.2 collective-permute-start.11
  196.5 2.4 collective-permute-done.9
  198.9 1.8 pad_maximum_fusion
  200.7 3.4 fusion.7
  204.1 56.0 %collective-permute-done.10 = bf16[1024,1408]{1,0:T(8,128)(2,1)} collective-permute-done((bf16[1024,1408]{1,0:T(8,128)(2,1)}, bf16[1024,1408]{1,0:T(8,128)(2,1)}, u32[]{:S(2)}, u32[]{:S(2)}) %collective-permute-start.10) | collective-permute-done | bytes 2883616 | tf_op jit(solution)/shard_map/ppermute | solution.py:27
  260.1 5.2 %fusion.4 = f32[1024,1408]{1,0:T(8,128)S(1)} fusion(bf16[1024,1408]{1,0:T(8,128)(2,1)} %collective-permute-done.10, bf16[1024,2048]{1,0:T(8,128)(2,1)S(1)} %bitcast.62), kind=kOutput, calls=%fused_computation.12 | convolution fusion | flops 2952790016 | bytes 10747904 | tf_op jit(solution)/shard_map/dot_general | solution.py:539
  265.4 56.1 %collective-permute-done.11 = bf16[1024,1408]{1,0:T(8,128)(2,1)} collective-permute-done((bf16[1024,1408]{1,0:T(8,128)(2,1)}, bf16[1024,1408]{1,0:T(8,128)(2,1)}, u32[]{:S(2)}, u32[]{:S(2)}) %collective-permute-start.11) | collective-permute-done | bytes 2883616 | tf_op jit(solution)/shard_map/ppermute | solution.py:27
  321.5 7.1 %fusion.2 = f32[1024,1408]{1,0:T(8,128)} fusion(bf16[1024,1408]{1,0:T(8,128)(2,1)} %collective-permute-done.11, bf16[1024,2048]{1,0:T(8,128)(2,1)S(1)} %bitcast.63), kind=kOutput, calls=%fused_computation.10 | convolution fusion | flops 2952790016 | bytes 10747904 | tf_op jit(solution)/shard_map/dot_general | solution.py:540
  328.5 6.2 %multiply_convert_fusion = bf16[1024,1408]{1,0:T(8,128)(2,1)S(1)} fusion(f32[1024,1408]{1,0:T(8,128)} %fusion.2, f32[1024,1408]{1,0:T(8,128)S(1)} %fusion.7, f32[1024,1408]{1,0:T(8,128)S(1)} %fusion.4, bf16[1024,1408]{1,0:T(8,128)(2,1)S(1)} %copy-done.8, bf16[1024,2048]{1,0:T(8,128)(2,1)S(1)} %bitcast.64), kind=kOutput, calls=%fused_computation | convolution fusion | flops 2964324352 | bytes 25165824 | tf_op jit(solution)/shard_map/dot_general | solution.py:538
  334.8 1.5 copy-done.14
  336.3 5.7 %convolution_convert_fusion = bf16[1024,1024]{1,0:T(8,128)(2,1)S(1)} fusion(bf16[1024,1408]{1,0:T(8,128)(2,1)S(1)} %multiply_convert_fusion, bf16[1024,1408]{1,0:T(8,128)(2,1)} %all-gather.11.cloned.1.call-done), kind=kOutput, calls=%fused_computation.8 | convolution fusion | flops 2953838592 | bytes 7864320 | tf_op jit(solution)/shard_map/dot_general | solution.py:544
  342.3 6.1 %convolution_convert_fusion.1 = bf16[1024,1024]{1,0:T(8,128)(2,1)S(1)} fusion(bf16[1024,1408]{1,0:T(8,128)(2,1)} %copy-done.14, bf16[1024,1408]{1,0:T(8,128)(2,1)} %all-gather.9.cloned.1.call-done), kind=kOutput, calls=%fused_computation.9 | convolution fusion | flops 2953838592 | bytes 7864320 | tf_op jit(solution)/shard_map/dot_general | solution.py:544
  348.6 0.5 collective-permute-start.13
  349.6 0.9 fusion.29
  350.4 1.5 collective-permute-start.16
  352.3 0.9 fusion.30
  353.2 1.0 collective-permute-start.14
  354.2 0.6 broadcast_in_dim.25.refs_5_
  354.8 10.4 %collective-permute-done.16 = bf16[1,256,1024]{2,1,0:T(8,128)(2,1)S(1)} collective-permute-done((bf16[1,256,1024]{2,1,0:T(8,128)(2,1)S(1)}, bf16[1,256,1024]{2,1,0:T(8,128)(2,1)S(1)}, u32[]{:S(2)}, u32[]{:S(2)}) %collective-permute-start.16) | collective-permute-done | bytes 524320 | tf_op jit(solution)/shard_map/ppermute | solution.py:27
  365.2 10.3 %collective-permute-done.14 = bf16[1,256,1024]{2,1,0:T(8,128)(2,1)S(1)} collective-permute-done((bf16[1,256,1024]{2,1,0:T(8,128)(2,1)S(1)}, bf16[1,256,1024]{2,1,0:T(8,128)(2,1)S(1)}, u32[]{:S(2)}, u32[]{:S(2)}) %collective-permute-start.14) | collective-permute-done | bytes 524320 | tf_op jit(solution)/shard_map/ppermute | solution.py:27
  375.5 0.8 copy-done.3
  376.3 4.4 %last.1 = bf16[256,2048]{1,0:T(8,128)(2,1)} custom-call(bf16[256,1024]{1,0:T(8,128)(2,1)} %get-tuple-element.26.refs_0_, bf16[256,1024]{1,0:T(8,128)(2,1)} %bitcast.79, bf16[256,1024]{1,0:T(8,128)(2,1)} %get-tuple-element.24.refs_2_, bf16[256,1024]{1,0:T(8,128)(2,1)} %bitcast.78, f32[256,2048]{1,0:T(8,128)} %get-tuple-element.12.refs_4_, ...), custom_call_target="tpu_custom_call" | custom-call | flops 1000000000 | bytes 5242880 | tf_op jit(solution)/shard_map/last/pallas_call | solution.py:548
  (62 shorter events, 2.2 us)
Async XLA Ops:
  6.5 14.2 %copy-start.11 = (f32[4]{0:T(128)S(1)}, f32[4]{0:T(128)}, u32[]{:S(2)}) copy-start(f32[4]{0:T(128)} %param.38) | copy-start | bytes 52
  6.5 14.2 %copy-start.10 = (f32[2]{0:T(128)S(1)}, f32[2]{0:T(128)}, u32[]{:S(2)}) copy-start(f32[2]{0:T(128)} %param.39) | copy-start | bytes 28
  6.5 187.9 %all-gather.5.cloned.1.call-start = ((), (), s32[]{:S(2)}) async-start(), calls=%async_computation | async-start | bytes 3604480 | tf_op jit(solution)/shard_map/all_gather | solution.py:354
  7.3 188.0 %all-gather.7.cloned.1.call-start = ((), (), s32[]{:S(2)}) async-start(), calls=%async_computation.1 | async-start | bytes 3604480 | tf_op jit(solution)/shard_map/all_gather | solution.py:355
  10.1 12.4 %collective-permute-start = (bf16[3,1024]{1,0:T(4,128)(2,1)S(1)}, bf16[3,1024]{1,0:T(4,128)(2,1)S(1)}, u32[]{:S(2)}, u32[]{:S(2)}) collective-permute-start(bf16[3,1024]{1,0:T(4,128)(2,1)S(1)} %pad_maximum_fusion.3), channel_id=1, source_target_pairs={{0,4},{4,8},{8,12},{12,16},{16,20},{20,24},{24,28},{1,5},{5,9},{9,... | collective-permute-start | bytes 18440 | tf_op jit(solution)/shard_map/ppermute | solution.py:27
  23.1 70.2 %copy-start.12 = (bf16[256]{0:T(256)(128)(2,1)S(1)}, bf16[256]{0:T(256)(128)(2,1)}, u32[]{:S(2)}) copy-start(bf16[256]{0:T(256)(128)(2,1)} %param.40) | copy-start | bytes 1540
  23.1 70.2 %copy-start.13 = (bf16[256]{0:T(256)(128)(2,1)S(1)}, bf16[256]{0:T(256)(128)(2,1)}, u32[]{:S(2)}) copy-start(bf16[256]{0:T(256)(128)(2,1)} %param.41) | copy-start | bytes 1540
  33.9 12.7 %collective-permute-start.1 = (bf16[144,512]{1,0:T(8,128)(2,1)}, bf16[144,512]{1,0:T(8,128)(2,1)S(1)}, u32[]{:S(2)}, u32[]{:S(2)}) collective-permute-start(bf16[144,512]{1,0:T(8,128)(2,1)} %get-tuple-element.10), channel_id=1, source_target_pairs={{0,16},{4,20},{8,24},{12,28},{1,17},{5,21},{9,25},{13,29},{2,18},{... | collective-permute-start | bytes 442376 | tf_op jit(solution)/shard_map/ppermute | solution.py:27
  38.4 14.0 %collective-permute-start.2 = (bf16[144,512]{1,0:T(8,128)(2,1)}, bf16[144,512]{1,0:T(8,128)(2,1)S(1)}, u32[]{:S(2)}, u32[]{:S(2)}) collective-permute-start(bf16[144,512]{1,0:T(8,128)(2,1)} %get-tuple-element.10), channel_id=1, source_target_pairs={{0,12},{4,16},{8,20},{12,24},{16,28},{1,13},{5,17},{9,21},{13,25},... | collective-permute-start | bytes 442376 | tf_op jit(solution)/shard_map/ppermute | solution.py:27
  40.6 17.6 %collective-permute-start.3 = (bf16[144,512]{1,0:T(8,128)(2,1)}, bf16[144,512]{1,0:T(8,128)(2,1)S(1)}, u32[]{:S(2)}, u32[]{:S(2)}) collective-permute-start(bf16[144,512]{1,0:T(8,128)(2,1)} %get-tuple-element.10), channel_id=1, source_target_pairs={{0,8},{4,12},{8,16},{12,20},{16,24},{20,28},{1,9},{5,13},{9,17},{1... | collective-permute-start | bytes 442376 | tf_op jit(solution)/shard_map/ppermute | solution.py:27
  43.2 15.1 %collective-permute-start.4 = (bf16[144,512]{1,0:T(8,128)(2,1)}, bf16[144,512]{1,0:T(8,128)(2,1)S(1)}, u32[]{:S(2)}, u32[]{:S(2)}) collective-permute-start(bf16[144,512]{1,0:T(8,128)(2,1)} %get-tuple-element.10), channel_id=1, source_target_pairs={{0,4},{4,8},{8,12},{12,16},{16,20},{20,24},{24,28},{1,5},{5,9},{9,... | collective-permute-start | bytes 442376 | tf_op jit(solution)/shard_map/ppermute | solution.py:27
  46.6 288.2 %all-gather.11.cloned.1.call-start = ((), (), s32[]{:S(2)}) async-start(), calls=%async_computation.3 | async-start | bytes 3604480 | tf_op jit(solution)/shard_map/all_gather | solution.py:361
  58.5 37.2 %collective-permute-start.5 = (bf16[130,512]{1,0:T(8,128)(2,1)S(1)}, bf16[130,512]{1,0:T(8,128)(2,1)S(1)}, u32[]{:S(2)}, u32[]{:S(2)}) collective-permute-start(bf16[130,512]{1,0:T(8,128)(2,1)S(1)} %pad_maximum_fusion.2), channel_id=1, source_target_pairs={{0,16},{4,20},{8,24},{12,28},{1,17},{5,21},{9,25},{13,29},{2,18},{... | collective-permute-start | bytes 399368 | tf_op jit(solution)/shard_map/ppermute | solution.py:27
  111.0 3.3 copy-start.1
  114.3 18.8 %collective-permute-start.6 = (bf16[2,256,2048]{2,1,0:T(8,128)(2,1)}, bf16[2,256,2048]{2,1,0:T(8,128)(2,1)S(1)}, u32[]{:S(2)}, u32[]{:S(2)}) collective-permute-start(bf16[2,256,2048]{2,1,0:T(8,128)(2,1)} %slice.164), channel_id=1, source_target_pairs={{0,1},{1,0},{2,3},{3,2},{4,5},{5,4},{6,7},{7,6},{8,9},{9,8},{10,11... | collective-permute-start | bytes 6291464 | tf_op jit(solution)/shard_map/ppermute | solution.py:27
  114.3 18.5 %collective-permute-start.12 = (bf16[256,1408]{1,0:T(8,128)(2,1)S(1)}, bf16[256,1408]{1,0:T(8,128)(2,1)S(1)}, u32[]{:S(2)}, u32[]{:S(2)}) collective-permute-start(bf16[256,1408]{1,0:T(8,128)(2,1)S(1)} %copy-done.1), channel_id=1, source_target_pairs={{0,4},{4,0},{1,5},{5,1},{2,6},{6,2},{3,7},{7,3},{8,12},{12,8},{9,1... | collective-permute-start | bytes 2162696 | tf_op jit(solution)/shard_map/ppermute | solution.py:27
  135.5 4.2 %copy-start.4 = (bf16[2048]{0:T(1024)(128)(2,1)S(1)}, bf16[2048]{0:T(1024)(128)(2,1)}, u32[]{:S(2)}) copy-start(bf16[2048]{0:T(1024)(128)(2,1)} %param.44) | copy-start | bytes 12292
  135.5 4.8 %copy-start.5 = (bf16[2048]{0:T(1024)(128)(2,1)S(1)}, bf16[2048]{0:T(1024)(128)(2,1)}, u32[]{:S(2)}) copy-start(bf16[2048]{0:T(1024)(128)(2,1)} %param.45) | copy-start | bytes 12292
  136.7 24.8 %collective-permute-start.7 = (bf16[1,256,2048]{2,1,0:T(8,128)(2,1)S(1)}, bf16[1,256,2048]{2,1,0:T(8,128)(2,1)S(1)}, u32[]{:S(2)}, u32[]{:S(2)}) collective-permute-start(bf16[1,256,2048]{2,1,0:T(8,128)(2,1)S(1)} %get-tuple-element.19), channel_id=1, source_target_pairs={{0,2},{1,3},{2,0},{3,1},{4,6},{5,7},{6,4},{7,5},{8,10},{9,11},{10,... | collective-permute-start | bytes 3145736 | tf_op jit(solution)/shard_map/ppermute | solution.py:27
  139.4 202.9 %all-gather.9.cloned.1.call-start = ((), (), s32[]{:S(2)}) async-start(), calls=%async_computation.2 | async-start | bytes 3604480 | tf_op jit(solution)/shard_map/all_gather | solution.py:361
  161.5 1.0 copy-start.9
  167.3 31.6 %copy-start = (bf16[256,2048]{1,0:T(8,128)(2,1)S(1)}, bf16[256,2048]{1,0:T(8,128)(2,1)}, u32[]{:S(2)}) copy-start(bf16[256,2048]{1,0:T(8,128)(2,1)} %get-tuple-element.11) | copy-start | bytes 3145732
  167.4 24.3 %collective-permute-start.8 = (bf16[1,256,2048]{2,1,0:T(8,128)(2,1)}, bf16[1,256,2048]{2,1,0:T(8,128)(2,1)S(1)}, u32[]{:S(2)}, u32[]{:S(2)}) collective-permute-start(bf16[1,256,2048]{2,1,0:T(8,128)(2,1)} %bitcast.67), channel_id=1, source_target_pairs={{0,2},{1,3},{2,0},{3,1},{4,6},{5,7},{6,4},{7,5},{8,10},{9,11},{10,... | collective-permute-start | bytes 3145736 | tf_op jit(solution)/shard_map/ppermute | solution.py:27
  194.4 4.5 %collective-permute-start.9 = (bf16[2,256,2048]{2,1,0:T(8,128)(2,1)}, bf16[2,256,2048]{2,1,0:T(8,128)(2,1)}, u32[]{:S(2)}, u32[]{:S(2)}) collective-permute-start(bf16[2,256,2048]{2,1,0:T(8,128)(2,1)} %pad_maximum_fusion.1), channel_id=1, source_target_pairs={{0,1},{1,0},{2,3},{3,2},{4,5},{5,4},{6,7},{7,6},{8,9},{9,8},{10,11... | collective-permute-start | bytes 6291464 | tf_op jit(solution)/shard_map/ppermute | solution.py:27
  194.4 65.7 %collective-permute-start.10 = (bf16[1024,1408]{1,0:T(8,128)(2,1)}, bf16[1024,1408]{1,0:T(8,128)(2,1)}, u32[]{:S(2)}, u32[]{:S(2)}) collective-permute-start(bf16[1024,1408]{1,0:T(8,128)(2,1)} %all-gather.5.cloned.1.call-done), channel_id=1, source_target_pairs={{0,4},{4,0},{1,5},{5,1},{2,6},{6,2},{3,7},{7,3},{8,12},{12,8},{9,1... | collective-permute-start | bytes 8650760 | tf_op jit(solution)/shard_map/ppermute | solution.py:27
  195.3 126.2 %collective-permute-start.11 = (bf16[1024,1408]{1,0:T(8,128)(2,1)}, bf16[1024,1408]{1,0:T(8,128)(2,1)}, u32[]{:S(2)}, u32[]{:S(2)}) collective-permute-start(bf16[1024,1408]{1,0:T(8,128)(2,1)} %all-gather.7.cloned.1.call-done), channel_id=1, source_target_pairs={{0,4},{4,0},{1,5},{5,1},{2,6},{6,2},{3,7},{7,3},{8,12},{12,8},{9,1... | collective-permute-start | bytes 8650760 | tf_op jit(solution)/shard_map/ppermute | solution.py:27
  196.5 4.2 %copy-start.7 = (bf16[1024,1408]{1,0:T(8,128)(2,1)S(1)}, bf16[1024,1408]{1,0:T(8,128)(2,1)}, u32[]{:S(2)}) copy-start(bf16[1024,1408]{1,0:T(8,128)(2,1)} %all-gather.5.cloned.1.call-done) | copy-start | bytes 8650756
  265.3 63.2 %copy-start.8 = (bf16[1024,1408]{1,0:T(8,128)(2,1)S(1)}, bf16[1024,1408]{1,0:T(8,128)(2,1)}, u32[]{:S(2)}) copy-start(bf16[1024,1408]{1,0:T(8,128)(2,1)} %all-gather.7.cloned.1.call-done) | copy-start | bytes 8650756
  334.7 1.6 copy-start.14
  342.2 7.0 %collective-permute-start.15 = (bf16[2,256,1024]{2,1,0:T(8,128)(2,1)S(1)}, bf16[2,256,1024]{2,1,0:T(8,128)(2,1)S(1)}, u32[]{:S(2)}, u32[]{:S(2)}) collective-permute-start(bf16[2,256,1024]{2,1,0:T(8,128)(2,1)S(1)} %bitcast.73), channel_id=1, source_target_pairs={{0,1},{1,0},{2,3},{3,2},{4,5},{5,4},{6,7},{7,6},{8,9},{9,8},{10,11... | collective-permute-start | bytes 3145736 | tf_op jit(solution)/shard_map/ppermute | solution.py:27
  348.6 3.3 collective-permute-start.13
  350.4 3.8 copy-start.6
  350.4 14.8 %collective-permute-start.16 = (bf16[1,256,1024]{2,1,0:T(8,128)(2,1)S(1)}, bf16[1,256,1024]{2,1,0:T(8,128)(2,1)S(1)}, u32[]{:S(2)}, u32[]{:S(2)}) collective-permute-start(bf16[1,256,1024]{2,1,0:T(8,128)(2,1)S(1)} %get-tuple-element.23), channel_id=1, source_target_pairs={{0,2},{1,3},{2,0},{3,1},{4,6},{5,7},{6,4},{7,5},{8,10},{9,11},{10,... | collective-permute-start | bytes 1572872 | tf_op jit(solution)/shard_map/ppermute | solution.py:27
  353.2 22.4 %collective-permute-start.14 = (bf16[1,256,1024]{2,1,0:T(8,128)(2,1)S(1)}, bf16[1,256,1024]{2,1,0:T(8,128)(2,1)S(1)}, u32[]{:S(2)}, u32[]{:S(2)}) collective-permute-start(bf16[1,256,1024]{2,1,0:T(8,128)(2,1)S(1)} %get-tuple-element.25), channel_id=1, source_target_pairs={{0,2},{1,3},{2,0},{3,1},{4,6},{5,7},{6,4},{7,5},{8,10},{9,11},{10,... | collective-permute-start | bytes 1572872 | tf_op jit(solution)/shard_map/ppermute | solution.py:27
  365.2 10.3 %copy-start.2 = (bf16[1,256,1024]{2,1,0:T(8,128)(2,1)}, bf16[1,256,1024]{2,1,0:T(8,128)(2,1)S(1)}, u32[]{:S(2)}) copy-start(bf16[1,256,1024]{2,1,0:T(8,128)(2,1)S(1)} %collective-permute-done.16) | copy-start | bytes 1572868
  375.5 0.8 copy-start.3
Sparse Core Ops, SparseCore 0:
  8.9 67.4 all-gather.4
  78.0 73.9 all-gather.6
  153.6 57.7 all-gather.10
  212.8 57.7 all-gather.8
